TPU v7x, 32 devices: a whole 2x2x4 slice. The times are simulated.
32 devices in a mesh: row: 16 (over z, y, x), col: 2 (over core).
Axes of the slice: x: 2, y: 2, z: 4, core: 2. Of those that a mesh axis runs over, the one named last changes fastest.
Arguments:
- tokens: bfloat16 [2, 3072, 2048], P('col', 'row'), may hold values from -6 to 6
- proj_in: bfloat16 [2048, 512], P('col'), may hold values from -0.125 to 0.125
- proj_out: bfloat16 [512, 2048], P(None, 'row'), may hold values from -0.25 to 0.25
Outputs:
- output: bfloat16 [2, 3072, 2048], P('col', 'row')
All inputs are finite; a program needn't handle non-finite values.
Results may differ from a plain program's by a relative error of at most 0.0083.
Values may be sent and summed in bfloat16 or wider, within the bound.
A program may use at most 64 MiB of HBM per device.

v0:
```python
import math
import jax
import jax.numpy as jnp
from jax import lax
from jax.sharding import PartitionSpec as P

GRP = 128
highest = lax.Precision.HIGHEST
span_inner = 128


def circle(height, breadth, period):
    product = lax.iota(jnp.int32, height)[:, None] * lax.iota(jnp.int32, breadth)[None, :] % period
    angle = product.astype(jnp.float32) * (2.0 * math.pi / period)
    return (jnp.cos(angle), jnp.sin(angle))


def positions(piece):
    real_in = piece[0, 0]
    imag_in = piece[1, 0]
    count, length = real_in.shape
    outer = length // span_inner
    real_in = real_in.reshape(count, outer, span_inner)
    imag_in = imag_in.reshape(count, outer, span_inner)
    cos_one, sin_one = circle(outer, outer, outer)
    first_re = jnp.einsum("ab,kbq->kaq", cos_one, real_in, precision=highest) - jnp.einsum(
        "ab,kbq->kaq", sin_one, imag_in, precision=highest
    )
    first_im = jnp.einsum("ab,kbq->kaq", sin_one, real_in, precision=highest) + jnp.einsum(
        "ab,kbq->kaq", cos_one, imag_in, precision=highest
    )
    twist_c, twist_s = circle(outer, span_inner, length)
    turned_re = first_re * twist_c - first_im * twist_s
    turned_im = first_re * twist_s + first_im * twist_c
    cos_two, sin_two = circle(span_inner, span_inner, span_inner)
    factor = 1.0 / math.sqrt(GRP * length)
    real_out = jnp.einsum("kaq,qb->kba", turned_re, cos_two, precision=highest) - jnp.einsum(
        "kaq,qb->kba", turned_im, sin_two, precision=highest
    )
    real_out = real_out.reshape(count, length) * factor
    return real_out[:, None, :]


def shards(tokens, proj_in, proj_out):
    seq_rows = tokens[0]
    local_len = seq_rows.shape[0]
    features = proj_in.shape[1]
    groups = features // GRP
    mapped = jnp.dot(
        seq_rows,
        lax.all_gather(proj_in, "col", axis=0, tiled=True),
        preferred_element_type=jnp.float32,
    ).astype(jnp.bfloat16)
    values = mapped.astype(jnp.float32).reshape(local_len, groups, GRP)
    cos_c, sin_c = circle(GRP, GRP, GRP)
    real_part = jnp.einsum("pgc,cs->gsp", values, cos_c, precision=highest)
    imag_part = jnp.einsum("pgc,cs->gsp", values, sin_c, precision=highest)
    ways = lax.axis_size("row")
    slots = groups * cos_c.shape[1]
    per_dev = slots // ways
    stacked = jnp.stack(
        [real_part.reshape(ways, per_dev, local_len), imag_part.reshape(ways, per_dev, local_len)],
        0,
    )
    spectra = positions(lax.all_to_all(stacked, "row", split_axis=1, concat_axis=3, tiled=True))
    outgoing = spectra.astype(jnp.bfloat16)
    back = lax.all_to_all(outgoing, "row", split_axis=2, concat_axis=0, tiled=True)
    mixed = back.reshape(features, local_len)
    result = lax.dot_general(
        mixed,
        lax.all_gather(proj_out, "row", axis=1, tiled=True),
        (((0,), (0,)), ((), ())),
        preferred_element_type=jnp.float32,
    )
    return result.astype(jnp.bfloat16)[None]


def solution(mesh):
    in_specs = (P("col", "row", None), P("col", None), P(None, "row"))
    out_specs = P("col", "row", None)
    return jax.shard_map(shards, mesh=mesh, in_specs=in_specs, out_specs=out_specs, check_vma=False)
```

profile of v0, /device:TPU:0, one launch (start us, length us, event | category | flops | bytes accessed | tf_op | source)
XLA Modules:
  0.0 115.2 jit_solution(4672272364211628046)
XLA Ops:
  6.5 0.7 all-gather.3.cloned.1.call-update
  7.3 0.7 all-gather.5.cloned.1.call-update
  8.0 14.2 %all-gather.3.cloned.1.call-done = bf16[2048,512]{1,0:T(8,128)(2,1)} async-done(((bf16[1024,512]{1,0:T(8,128)(2,1)}), bf16[2048,512]{1,0:T(8,128)(2,1)}) %all-gather.3.cloned.1.call-update) | async-done | bytes 2097168 | tf_op jit(solution)/shard_map/all_gather | solution.py:51
  22.2 2.2 %fusion.5 = bf16[24,4,8,128]{3,2,1,0:T(8,128)(2,1)S(1)} fusion(bf16[2048,512]{1,0:T(8,128)(2,1)} %all-gather.3.cloned.1.call-done, bf16[1,192,2048]{2,1,0:T(8,128)(2,1)S(1)} %copy-done), kind=kOutput, calls=%fused_computation.12 | convolution fusion | flops 402751488 | bytes 3080192 | tf_op jit(solution)/shard_map/dot_general | solution.py:49
  24.4 0.6 convolution_bitcast_fusion.1
  24.9 0.2 copy.19
  25.2 0.6 convolution_bitcast_fusion
  25.7 0.2 copy.21
  26.0 1.1 copy.22
  27.1 6.8 %all-to-all-start = ((f32[2,16,32,192]{3,2,0,1:T(8,128)}), f32[2,16,32,192]{3,2,0,1:T(8,128)S(1)}, u32[]{:S(2)}, u32[]{:S(2)}) async-start(f32[2,16,32,192]{3,2,0,1:T(8,128)} %copy.22), calls=%async_computation | async-start | bytes 2097152 | tf_op jit(solution)/shard_map/all_to_all | solution.py:65
  34.0 24.7 %all-to-all-done = f32[2,16,32,192]{3,2,0,1:T(8,128)S(1)} async-done(((f32[2,16,32,192]{3,2,0,1:T(8,128)}), f32[2,16,32,192]{3,2,0,1:T(8,128)S(1)}, u32[]{:S(2)}, u32[]{:S(2)}) %all-to-all-start) | async-done | bytes 786464 | tf_op jit(solution)/shard_map/all_to_all | solution.py:65
  58.7 0.1 fusion.95
  58.8 0.3 copy.23
  59.1 0.3 reshape_squeeze.6
  59.4 0.3 copy.24
  59.7 0.3 reshape_squeeze.7
  60.0 0.5 fusion.39
  60.5 0.5 fusion.35
  61.0 0.5 fusion.2
  61.6 0.6 multiply_add_fusion
  62.2 0.7 fusion.9
  62.9 0.7 fusion.6
  63.7 0.4 copy.31
  64.1 0.4 reshape.66
  64.5 0.5 broadcast.106
  65.0 17.0 %reduce = bf16[3072,32]{1,0:T(8,128)(2,1)S(1)} reduce(bf16[3072,1,32]{2,1,0:T(2,128)(2,1)S(1)} %bitcast.68, bf16[]{:T(256)} %broadcast.106), dimensions={1}, to_apply=%bitcast.57.reduce_sub_computation | reduce | bytes 393218
  82.0 0.8 reshape.67
  82.7 19.8 %all_to_all.30 = bf16[16,2,3072]{2,1,0:T(2,128)(2,1)S(1)} all-to-all(bf16[16,2,3072]{2,1,0:T(2,128)(2,1)S(1)} %reshape.67), channel_id=1, replica_groups=mesh['row'=16,'col'=2] {'row'}, dimensions={0} | all-to-all | bytes 393216 | tf_op jit(solution)/shard_map/all_to_all | solution.py:67
  102.6 0.9 reshape.68
  103.4 1.4 %copy.29 = bf16[32,1,3072]{2,0,1:T(8,128)(2,1)S(1)} copy(bf16[32,1,3072]{0,1,2:T(2,128)(2,1)S(1)} %bitcast.69) | data formatting | bytes 393216 | tf_op jit(solution)/shard_map/all_to_all | solution.py:67
  104.8 0.3 all_to_all.26
  105.2 3.1 %fusion = bf16[1,192,2048]{2,1,0:T(8,128)(2,1)} fusion(bf16[512,192]{1,0:T(8,128)(2,1)S(1)} %bitcast.73, bf16[512,2048]{1,0:T(8,128)(2,1)} %all-gather.5.cloned.1.call-done), kind=kOutput, calls=%fused_computation.1 | convolution fusion | flops 403046400 | bytes 3080192 | tf_op jit(solution)/shard_map/dot_general | solution.py:69
  (8 shorter events, 0.3 us)
Async XLA Ops:
  6.5 15.7 %copy-start = (bf16[1,192,2048]{2,1,0:T(8,128)(2,1)S(1)}, bf16[1,192,2048]{2,1,0:T(8,128)(2,1)}, u32[]{:S(2)}) copy-start(bf16[1,192,2048]{2,1,0:T(8,128)(2,1)} %param.3) | copy-start | bytes 2359300
  6.5 15.7 %all-gather.3.cloned.1.call-start = ((), (), s32[]{:S(2)}) async-start(), calls=%async_computation.2 | async-start | bytes 3145728 | tf_op jit(solution)/shard_map/all_gather | solution.py:51
  7.3 98.0 %all-gather.5.cloned.1.call-start = ((), (), s32[]{:S(2)}) async-start(), calls=%async_computation.3 | async-start | bytes 2228224 | tf_op jit(solution)/shard_map/all_gather | solution.py:71
  27.1 31.6 %all-to-all-start = ((f32[2,16,32,192]{3,2,0,1:T(8,128)}), f32[2,16,32,192]{3,2,0,1:T(8,128)S(1)}, u32[]{:S(2)}, u32[]{:S(2)}) async-start(f32[2,16,32,192]{3,2,0,1:T(8,128)} %copy.22), calls=%async_computation | async-start | bytes 2097152 | tf_op jit(solution)/shard_map/all_to_all | solution.py:65
Sparse Core Ops, SparseCore 0:
  8.9 13.2 all-gather.2
  24.9 73.4 all-gather.4
where the time goes:
time: 115 us
  waiting for transfers between devices  40.3 us (35%)
  blocking collectives  19.8 us (17%)
  other arithmetic  17.1 us (15%)
  between operations  13.6 us (12%)
  matrix products  10 us (9%)
  local copies, waits for them, and re-layouts  7.43 us (6%)
  starting transfers between devices  6.84 us (6%)
    all_to_all x1, waiting for transfers between devices, shards(): lax.all_to_all(stacked, 'row', split_axis=1, concat_axis=3, tiled=True)  24.7 us
    all_to_all x1, blocking collectives, shards(): lax.all_to_all(outgoing, 'row', split_axis=2, concat_axis=0, tiled=True)  19.8 us
    unnamed x1, other arithmetic  17 us
    all_gather x1, waiting for transfers between devices, shards(): lax.all_gather(proj_in, 'col', axis=0, tiled=True)  14.2 us
    all_to_all x1, starting transfers between devices, shards(): lax.all_to_all(stacked, 'row', split_axis=1, concat_axis=3, tiled=True)  6.8 us
    dot_general x1, matrix products, shards(): lax.dot_general(mixed, lax.all_gather(proj_out, 'row', axis=1, tiled=True...  3.08 us
  transfers between devices with their start and end apart: 3, of which 2 were waited for; matrix products, arithmetic and copies ran while one was open for 27% of the time, Pallas kernels for 0%

commit v1 on v0

--- a/solution.py
+++ b/solution.py
@@ -62,7 +62,14 @@
         [real_part.reshape(ways, per_dev, local_len), imag_part.reshape(ways, per_dev, local_len)],
         0,
     )
-    spectra = positions(lax.all_to_all(stacked, "row", split_axis=1, concat_axis=3, tiled=True))
+    spectra = positions(
+        jnp.concatenate(
+            lax.all_to_all(
+                jnp.stack(jnp.split(stacked, lax.axis_size("row"), axis=1)), "row", 0, 0
+            ),
+            3,
+        )
+    )
     outgoing = spectra.astype(jnp.bfloat16)
     back = lax.all_to_all(outgoing, "row", split_axis=2, concat_axis=0, tiled=True)
     mixed = back.reshape(features, local_len)

time: 115 us -> 127 us (1.10)
  other arithmetic: 17.1 us -> 27 us
  waiting for transfers between devices: 40.3 us -> 48.6 us
  blocking collectives: 19.8 us -> 13.9 us
    unnamed x1 -> x16, other arithmetic: 17 us -> 26.4 us
    all_to_all x1, waiting for transfers between devices: 24.7 us -> 33 us  [shards(): lax.all_to_all(jnp.stack(jnp.split(stacked, lax.axis_size('row'), axis=1)...]
    all_to_all x1, blocking collectives: 19.8 us -> 13.9 us  [shards(): lax.all_to_all(outgoing, 'row', split_axis=2, concat_axis=0, tiled=True)]
  transfers between devices with their start and end apart: 3 -> 3, of which waited for: 2 -> 2; matrix products, arithmetic and copies ran while one was open for 27% -> 32% of each run, Pallas kernels for 0% -> 0%
where the time goes in v1:
time: 127 us; the launch traced here: 126 us
  waiting for transfers between devices  48.6 us (38%)
  other arithmetic  27 us (21%)
  blocking collectives  13.9 us (11%)
  between operations  13.6 us (11%)
  matrix products  10 us (8%)
  starting transfers between devices  6.84 us (5%)
  local copies, waits for them, and re-layouts  6.34 us (5%)
    all_to_all x1, waiting for transfers between devices, shards(): lax.all_to_all(jnp.stack(jnp.split(stacked, lax.axis_size('row'), axis=1)...  33 us
    unnamed x16, other arithmetic  26.4 us
    all_gather x1, waiting for transfers between devices, shards(): lax.all_gather(proj_in, 'col', axis=0, tiled=True)  14.2 us
    all_to_all x1, blocking collectives, shards(): lax.all_to_all(outgoing, 'row', split_axis=2, concat_axis=0, tiled=True)  13.9 us
    all_to_all x1, starting transfers between devices, shards(): lax.all_to_all(jnp.stack(jnp.split(stacked, lax.axis_size('row'), axis=1)...  6.8 us
    dot_general x1, matrix products, shards(): lax.dot_general(mixed, lax.all_gather(proj_out, 'row', axis=1, tiled=True...  3.08 us
  transfers between devices with their start and end apart: 3, of which 2 were waited for; matrix products, arithmetic and copies ran while one was open for 32% of the time, Pallas kernels for 0%

profile of v1, /device:TPU:0, one launch (start us, length us, event | category | flops | bytes accessed | tf_op | source)
XLA Modules:
  0.0 126.4 jit_solution(7654711350104280932)
XLA Ops:
  6.5 0.7 all-gather.3.cloned.1.call-update
  7.3 0.7 all-gather.5.cloned.1.call-update
  8.0 14.2 %all-gather.3.cloned.1.call-done = bf16[2048,512]{1,0:T(8,128)(2,1)} async-done(((bf16[1024,512]{1,0:T(8,128)(2,1)}), bf16[2048,512]{1,0:T(8,128)(2,1)}) %all-gather.3.cloned.1.call-update) | async-done | bytes 2097168 | tf_op jit(solution)/shard_map/all_gather | solution.py:51
  22.2 2.2 %fusion.5 = bf16[24,4,8,128]{3,2,1,0:T(8,128)(2,1)S(1)} fusion(bf16[2048,512]{1,0:T(8,128)(2,1)} %all-gather.3.cloned.1.call-done, bf16[1,192,2048]{2,1,0:T(8,128)(2,1)S(1)} %copy-done), kind=kOutput, calls=%fused_computation.42 | convolution fusion | flops 402751488 | bytes 3080192 | tf_op jit(solution)/shard_map/dot_general | solution.py:49
  24.9 0.6 convolution_bitcast_fusion
  25.9 0.6 bitcast_dynamic-update-slice_fusion.14
  26.6 0.6 bitcast_dynamic-update-slice_fusion.13
  27.2 0.6 bitcast_dynamic-update-slice_fusion.12
  27.8 0.6 bitcast_dynamic-update-slice_fusion.11
  28.4 0.6 bitcast_dynamic-update-slice_fusion.10
  29.1 0.6 bitcast_dynamic-update-slice_fusion.9
  29.7 0.6 bitcast_dynamic-update-slice_fusion.8
  30.3 0.6 bitcast_dynamic-update-slice_fusion.7
  30.9 0.6 bitcast_dynamic-update-slice_fusion.6
  31.6 0.6 bitcast_dynamic-update-slice_fusion.5
  32.2 0.6 bitcast_dynamic-update-slice_fusion.4
  32.8 0.6 bitcast_dynamic-update-slice_fusion.3
  33.4 0.6 bitcast_dynamic-update-slice_fusion.2
  34.1 0.6 bitcast_dynamic-update-slice_fusion.1
  34.7 0.6 bitcast_dynamic-update-slice_fusion
  35.3 0.6 fusion.34
  35.9 6.8 %all-to-all-start = ((f32[16,2,1,32,192]{4,3,1,2,0:T(8,128)}), f32[16,2,1,32,192]{4,3,1,2,0:T(8,128)S(1)}, u32[]{:S(2)}, u32[]{:S(2)}) async-start(f32[16,2,1,32,192]{4,3,1,2,0:T(8,128)} %fusion.34), calls=%async_computation | async-start | bytes 2097152 | tf_op jit(solution)/shard_map/all_to_all | solution.py:67
  42.8 33.0 %all-to-all-done = f32[16,2,1,32,192]{4,3,1,2,0:T(8,128)S(1)} async-done(((f32[16,2,1,32,192]{4,3,1,2,0:T(8,128)}), f32[16,2,1,32,192]{4,3,1,2,0:T(8,128)S(1)}, u32[]{:S(2)}, u32[]{:S(2)}) %all-to-all-start) | async-done | bytes 786464 | tf_op jit(solution)/shard_map/all_to_all | solution.py:67
  78.7 0.6 multiply_add_fusion
  79.3 0.7 fusion.9
  80.1 0.7 fusion.6
  82.2 17.0 %reduce = bf16[3072,32]{1,0:T(8,128)(2,1)S(1)} reduce(bf16[3072,1,32]{2,1,0:T(2,128)(2,1)S(1)} %bitcast.162, bf16[]{:T(256)} %broadcast.106), dimensions={1}, to_apply=%bitcast.119.reduce_sub_computation | reduce | bytes 393218
  99.1 0.8 reshape.72
  99.9 13.9 %all_to_all.20 = bf16[16,2,3072]{2,1,0:T(2,128)(2,1)S(1)} all-to-all(bf16[16,2,3072]{2,1,0:T(2,128)(2,1)S(1)} %reshape.72), channel_id=1, replica_groups=mesh['row'=16,'col'=2] {'row'}, dimensions={0} | all-to-all | bytes 393216 | tf_op jit(solution)/shard_map/all_to_all | solution.py:74
  113.8 0.9 reshape.73
  114.7 1.4 %copy.73 = bf16[32,1,3072]{2,0,1:T(8,128)(2,1)S(1)} copy(bf16[32,1,3072]{0,1,2:T(2,128)(2,1)S(1)} %bitcast.163) | data formatting | bytes 393216 | tf_op jit(solution)/shard_map/all_to_all | solution.py:74
  116.5 3.1 %fusion = bf16[1,192,2048]{2,1,0:T(8,128)(2,1)} fusion(bf16[512,192]{1,0:T(8,128)(2,1)S(1)} %bitcast.165, bf16[512,2048]{1,0:T(8,128)(2,1)} %all-gather.5.cloned.1.call-done), kind=kOutput, calls=%fused_computation.31 | convolution fusion | flops 403046400 | bytes 3080192 | tf_op jit(solution)/shard_map/dot_general | solution.py:76
  (22 shorter events, 5.6 us)
Async XLA Ops:
  6.5 15.7 %copy-start = (bf16[1,192,2048]{2,1,0:T(8,128)(2,1)S(1)}, bf16[1,192,2048]{2,1,0:T(8,128)(2,1)}, u32[]{:S(2)}) copy-start(bf16[1,192,2048]{2,1,0:T(8,128)(2,1)} %param.3) | copy-start | bytes 2359300
  6.5 15.7 %all-gather.3.cloned.1.call-start = ((), (), s32[]{:S(2)}) async-start(), calls=%async_computation.2 | async-start | bytes 3145728 | tf_op jit(solution)/shard_map/all_gather | solution.py:51
  7.3 109.2 %all-gather.5.cloned.1.call-start = ((), (), s32[]{:S(2)}) async-start(), calls=%async_computation.3 | async-start | bytes 2228224 | tf_op jit(solution)/shard_map/all_gather | solution.py:78
  35.9 39.9 %all-to-all-start = ((f32[16,2,1,32,192]{4,3,1,2,0:T(8,128)}), f32[16,2,1,32,192]{4,3,1,2,0:T(8,128)S(1)}, u32[]{:S(2)}, u32[]{:S(2)}) async-start(f32[16,2,1,32,192]{4,3,1,2,0:T(8,128)} %fusion.34), calls=%async_computation | async-start | bytes 2097152 | tf_op jit(solution)/shard_map/all_to_all | solution.py:67
Sparse Core Ops, SparseCore 0:
  8.9 13.2 all-gather.2
  24.9 74.8 all-gather.4
